TPU v7x, 32 devices: a whole 2x2x4 slice. The times are simulated.
32 devices in a mesh: sp: 16 (over z, y, x), dp: 2 (over core).
Axes of the slice: x: 2, y: 2, z: 4, core: 2. Of those that a mesh axis runs over, the one named last changes fastest.
Arguments:
- glu_value: bfloat16 [2, 8192, 512], P('dp', 'sp'), may hold values from -6 to 6
- glu_gate: bfloat16 [2, 8192, 512], P('dp', 'sp'), may hold values from -8 to 8
- cotangent: bfloat16 [2, 8192, 2048], P('dp', 'sp'), may hold values from -8 to 8
- conv_weight: float32 [31, 512], replicated, may hold values from -1 to 1
- norm_gain: float32 [512], replicated, may hold values from 0.1 to 1.9
- norm_shift: float32 [512], replicated, may hold values from -3 to 3
- out_weight: bfloat16 [2048, 512], P('dp'), may hold values from -0.25 to 0.25
Outputs:
- grad_value: bfloat16 [2, 8192, 512], P('dp', 'sp')
- grad_gate: bfloat16 [2, 8192, 512], P('dp', 'sp')
- grad_out_weight: float32 [2048, 512], P('dp')
- grad_conv: float32 [31, 512], replicated
- grad_gain: float32 [512], replicated
- grad_shift: float32 [512], replicated
All inputs are finite; a program needn't handle non-finite values.
Results may differ from a plain program's by a relative error of at most 0.003.
Values may be sent and summed in bfloat16 or wider, within the bound.
No kernel may reach another device: no remote copies, remote signals or barrier semaphores. Data moves between devices by JAX's collectives and lax.ppermute only.
A program may use at most 64 MiB of HBM per device.

v0:
```python
import math
import jax
import jax.numpy as jnp
from jax import lax
from jax.sharding import PartitionSpec as P

epsilon = 1e-06


def from_behind(value, axis, by):
    count = lax.axis_size(axis)
    pairs = [(i, i + by) for i in range(count) if 0 <= i + by < count]
    return lax.ppermute(value, axis, pairs)


def per_device(glu_value, glu_gate, cotangent, conv_weight, norm_gain, norm_shift, out_weight):
    value_rows = glu_value[0]
    gate_rows = glu_gate[0]
    cotan_rows = cotangent[0]
    length = value_rows.shape[0]
    channels = value_rows.shape[1]
    tap_count = conv_weight.shape[0]
    halo_rows = tap_count - 1
    count_sp = lax.axis_size("sp")
    count_dp = lax.axis_size("dp")
    scale = 1.0 / math.sqrt(length * count_sp * count_dp)
    prior_value, prior_gate = from_behind(
        (value_rows[length - halo_rows :], gate_rows[length - halo_rows :]), "sp", 1
    )
    value_ext = jnp.concatenate([prior_value, value_rows], axis=0).astype(jnp.float32)
    gate_ext = jnp.concatenate([prior_gate, gate_rows], axis=0).astype(jnp.float32)
    gated_ext = value_ext * jax.nn.sigmoid(gate_ext)
    conv_rows = jnp.zeros((length, channels), jnp.float32)
    for offset in range(tap_count):
        conv_rows = conv_rows + conv_weight[offset] * gated_ext[offset : offset + length]
    centred = conv_rows - jnp.mean(conv_rows, axis=-1, keepdims=True)
    inv_std = lax.rsqrt(jnp.mean(centred * centred, axis=-1, keepdims=True) + epsilon)
    normed = centred * inv_std
    pre_act = normed * norm_gain + norm_shift
    sigmoid_pre = jax.nn.sigmoid(pre_act)
    act_rows = (pre_act * sigmoid_pre).astype(jnp.bfloat16)
    columns = cotan_rows
    grad_act = jnp.dot(
        columns,
        lax.all_gather(out_weight, "dp", axis=0, tiled=True),
        preferred_element_type=jnp.float32,
    )
    grad_pre = grad_act * sigmoid_pre * (1.0 + pre_act * (1.0 - sigmoid_pre))
    grad_normed = grad_pre * norm_gain
    grad_conv_rows = inv_std * (
        grad_normed
        - jnp.mean(grad_normed, axis=-1, keepdims=True)
        - normed * jnp.mean(grad_normed * normed, axis=-1, keepdims=True)
    )
    later_grads = from_behind(grad_conv_rows[:halo_rows], "sp", -1)
    padded_grad = jnp.concatenate([grad_conv_rows, later_grads], axis=0)
    grad_gated = jnp.zeros((length, channels), jnp.float32)
    for offset in range(tap_count):
        start = tap_count - 1 - offset
        grad_gated = grad_gated + conv_weight[offset] * padded_grad[start : start + length]
    grad_taps = jnp.stack(
        [
            jnp.sum(grad_conv_rows * gated_ext[offset : offset + length], axis=0)
            for offset in range(tap_count)
        ],
        axis=0,
    )
    sigmoid_gate = jax.nn.sigmoid(gate_ext[halo_rows:])
    grad_value = (grad_gated * sigmoid_gate).astype(jnp.bfloat16)
    grad_gate = (grad_gated * value_ext[halo_rows:] * sigmoid_gate * (1.0 - sigmoid_gate)).astype(
        jnp.bfloat16
    )
    grad_conv, grad_gain, grad_shift = lax.psum(
        (
            grad_taps * scale,
            jnp.sum(grad_pre * normed, axis=0) * scale,
            jnp.sum(grad_pre, axis=0) * scale,
        ),
        ("sp", "dp"),
    )
    columns = cotan_rows
    product = lax.dot_general(
        columns, act_rows, (((0,), (0,)), ((), ())), preferred_element_type=jnp.float32
    )
    partial_rows = lax.psum_scatter(product * scale, "dp", scatter_dimension=0, tiled=True)
    grad_out_weight = lax.psum(partial_rows, "sp")
    return (grad_value[None], grad_gate[None], grad_out_weight, grad_conv, grad_gain, grad_shift)


def solution(mesh):
    in_specs = (
        P("dp", "sp", None),
        P("dp", "sp", None),
        P("dp", "sp", None),
        P(),
        P(),
        P(),
        P("dp", None),
    )
    out_specs = (P("dp", "sp", None), P("dp", "sp", None), P("dp", None), P(), P(), P())
    return jax.shard_map(
        per_device, mesh=mesh, in_specs=in_specs, out_specs=out_specs, check_vma=False
    )
```

profile of v0, /device:TPU:8, one launch (start us, length us, event | category | flops | bytes accessed | tf_op | source)
XLA Modules:
  0.0 316.3 jit_solution(10922288983692130966)
XLA Ops:
  7.2 0.0 copy-start
  7.2 0.0 copy-start.5
  7.2 0.0 all-gather.2.cloned.1.call-start
  7.2 0.7 all-gather.2.cloned.1.call-update
  7.9 0.0 reduce-scatter.2.cloned.1.call-start
  8.0 0.8 slice_bitcast_fusion
  8.7 3.4 %collective-permute-start.1 = (bf16[30,512]{1,0:T(8,128)(2,1)S(1)}, bf16[30,512]{1,0:T(8,128)(2,1)S(1)}, u32[]{:S(2)}, u32[]{:S(2)}) collective-permute-start(bf16[30,512]{1,0:T(8,128)(2,1)S(1)} %slice_bitcast_fusion), channel_id=1, source_target_pairs={{0,2},{2,4},{4,6},{6,8},{8,10},{10,12},{12,14},{14,16},{16,18},{18... | collective-permute-start | bytes 92168 | tf_op jit(solution)/shard_map/ppermute | solution.py:13
  12.2 0.8 slice_bitcast_fusion.1
  12.9 3.4 %collective-permute-start = (bf16[30,512]{1,0:T(8,128)(2,1)S(1)}, bf16[30,512]{1,0:T(8,128)(2,1)S(1)}, u32[]{:S(2)}, u32[]{:S(2)}) collective-permute-start(bf16[30,512]{1,0:T(8,128)(2,1)S(1)} %slice_bitcast_fusion.1), channel_id=1, source_target_pairs={{0,2},{2,4},{4,6},{6,8},{8,10},{10,12},{12,14},{14,16},{16,18},{18... | collective-permute-start | bytes 92168 | tf_op jit(solution)/shard_map/ppermute | solution.py:13
  16.3 0.0 copy-done.5
  16.4 0.0 collective-permute-done.1
  16.4 4.1 %collective-permute-done = bf16[30,512]{1,0:T(8,128)(2,1)S(1)} collective-permute-done((bf16[30,512]{1,0:T(8,128)(2,1)S(1)}, bf16[30,512]{1,0:T(8,128)(2,1)S(1)}, u32[]{:S(2)}, u32[]{:S(2)}) %collective-permute-start) | collective-permute-done | bytes 30752 | tf_op jit(solution)/shard_map/ppermute | solution.py:13
  20.5 1.6 divide_multiply_fusion
  22.1 0.0 copy-start.6
  22.2 0.0 copy-start.7
  22.2 5.0 %fusion.113 = (f32[512]{0:T(512)S(1)}, f32[512,512]{1,0:T(8,128)S(1)}) fusion(f32[542,512]{1,0:T(8,128)S(1)} %divide_multiply_fusion, f32[512]{0:T(512)S(1)} %bitcast.148, f32[512]{0:T(512)S(1)} %bitcast.150, f32[512]{0:T(512)S(1)} %bitcast.92, f32[512]{0:T(512)S(1)} %bitcast.94, f32[512]{0:T(512)S(1)} %bitcast.96, f32[512]{0:T(512)S(1)} %bitcast.98, ...), kind=kLoop, calls=%fused_computation.212 | loop fusion | flops 16252416 | bytes 33619968 | tf_op jit(solution)/shard_map/reduce_sum | solution.py:36
  27.2 0.0 copy-start.2
  27.2 0.3 multiply_reduce_fusion.33
  27.4 0.7 copy-done.2
  28.1 0.0 copy-done
  28.1 0.0 copy-done.6
  28.1 0.0 copy-done.7
  28.1 3.4 %multiply_bitcast_fusion = f32[2048,512]{0,1:T(8,128)} fusion(bf16[1,512,2048]{2,1,0:T(8,128)(2,1)S(1)} %copy-done, f32[512,512]{1,0:T(8,128)S(1)} %get-tuple-element.54, f32[512]{0:T(512)S(1)} %copy-done.7, f32[512]{0:T(512)S(1)} %copy-done.6, f32[512]{0:T(512)S(1)} %add_rsqrt_fusion, f32[512]{0:T(512)S(1)} %broadcast_multiply_fusion.5), kind=kOutput, calls=%fused_computation.29 | convolution fusion | flops 1077149696 | bytes 7348224 | tf_op jit(solution)/shard_map/dot_general | solution.py:82
  31.5 0.0 reduce-scatter.2.cloned.1.call-update
  31.5 0.0 all-reduce.4.cloned.1.call-start
  31.6 0.0 copy-start.4
  31.6 2.4 maximum_convert_fusion.1
  34.0 0.0 copy-done.4
  34.0 1.2 maximum_convert_fusion
  35.1 0.0 all-gather.2.cloned.1.call-done
  35.1 5.1 %multiply_reduce_fusion = (f32[512]{0:T(512)}, f32[512]{0:T(512)S(1)}, f32[512]{0:T(512)S(1)}, f32[512]{0:T(512)}, f32[512,512]{1,0:T(8,128)}) fusion(f32[512,512]{1,0:T(8,128)} %copy-done.2, f32[512]{0:T(512)S(1)} %add_rsqrt_fusion, f32[512]{0:T(512)S(1)} %broadcast_multiply_fusion.5, f32[512]{0:T(512)S(1)} %copy-done.6, f32[512]{0:T(512)S(1)} %copy-done.7, ...), kind=kOutput, calls=%fused_computation.151 | convolution fusion | flops 1078720512 | bytes 6307840 | tf_op jit(solution)/shard_map/dot_general | solution.py:43
  40.2 3.1 reduce-scatter.2.cloned.1.call-done
  43.3 0.0 all-reduce.4.cloned.1.call-update
  43.3 0.0 all-reduce.6.cloned.1.call-start
  43.4 4.2 %multiply_reduce_fusion.1 = (f32[512]{0:T(512)S(1)}, f32[512]{0:T(512)S(1)}, f32[512]{0:T(512)S(1)}, f32[512]{0:T(512)S(1)}, f32[512]{0:T(512)S(1)}, /*index=5*/...) fusion(f32[542,512]{1,0:T(8,128)S(1)} %divide_multiply_fusion, ...), kind=kLoop, calls=%fused_computation.152 | loop fusion | flops 11262976 | bytes 22067200 | tf_op jit(solution)/shard_map/reduce_sum | solution.py:63
  47.6 0.0 copy-start.1
  47.6 4.5 %collective-permute-start.2 = (f32[30,512]{1,0:T(8,128)S(1)}, f32[30,512]{1,0:T(8,128)S(1)}, u32[]{:S(2)}, u32[]{:S(2)}) collective-permute-start(f32[30,512]{1,0:T(8,128)S(1)} %slice.489), channel_id=1, source_target_pairs={{2,0},{4,2},{6,4},{8,6},{10,8},{12,10},{14,12},{16,14},{18,16},{20... | collective-permute-start | bytes 184328 | tf_op jit(solution)/shard_map/ppermute | solution.py:13
  52.0 2.3 multiply_reduce_fusion.19
  54.4 0.0 copy-done.1
  54.4 1.6 stack.127
  56.0 0.6 broadcast_multiply_fusion
  56.6 1.3 broadcast_multiply_fusion.1
  57.9 0.0 all-reduce.6.cloned.1.call-update
  57.9 0.0 copy-start.3
  57.9 0.0 collective-permute-done.2
  57.9 23.0 %fusion.105 = (bf16[1,512,512]{2,1,0:T(8,128)(2,1)}, f32[512,512]{1,0:T(8,128)S(1)}) fusion(f32[542,512]{1,0:T(8,128)} %maximum_convert_fusion, f32[542,512]{1,0:T(8,128)} %maximum_convert_fusion.1, f32[512,512]{1,0:T(8,128)} %copy-done.1, f32[512]{0:T(512)S(1)} %bitcast.149, f32[30,512]{1,0:T(8,128)S(1)} %collective-permute-done.2, f32[512]{0:T(512)S(1)} %bitcast.151, ...), kind=kLoop, calls=%fused_computation.196 | loop fusion | flops 25952256 | bytes 4843520 | tf_op jit(solution)/shard_map/broadcast_in_dim | solution.py:87
  81.0 0.0 copy-done.3
  81.0 1.1 fusion.104
  82.1 94.1 %all-reduce.4.cloned.1.call-done = f32[1024,512]{0,1:T(8,128)} async-done(((f32[1024,512]{0,1:T(8,128)}), f32[1024,512]{0,1:T(8,128)}) %all-reduce.4.cloned.1.call-update) | async-done | bytes 2097168 | tf_op jit(solution)/shard_map/psum | solution.py:86
  176.1 2.9 copy.13
  179.0 126.8 %all-reduce.6.cloned.1.call-done = (f32[31,512]{1,0:T(8,128)}, f32[512]{0:T(512)}, f32[512]{0:T(512)}) async-done(((f32[31,512]{1,0:T(8,128)}, f32[512]{0:T(512)}, f32[512]{0:T(512)}), (f32[31,512]{1,0:T(8,128)}, f32[512]{0:T(512)}, f32[512]{0:T(512)})) %all-reduce.6.cloned.1.call-update) | async-done | bytes 67600 | tf_op jit(solution)/shard_map/psum | solution.py:73
  305.8 1.5 copy.18
  307.3 1.3 copy.19
  308.6 1.2 copy.20
  (6 shorter events, 0.1 us)
Async XLA Ops:
  7.2 20.9 %copy-start = (bf16[1,512,2048]{2,1,0:T(8,128)(2,1)S(1)}, bf16[1,512,2048]{2,1,0:T(8,128)(2,1)}, u32[]{:S(2)}) copy-start(bf16[1,512,2048]{2,1,0:T(8,128)(2,1)} %param.9) | copy-start | bytes 6291460
  7.2 9.2 %copy-start.5 = (f32[31,512]{1,0:T(8,128)S(1)}, f32[31,512]{1,0:T(8,128)}, u32[]{:S(2)}) copy-start(f32[31,512]{1,0:T(8,128)} %param.10) | copy-start | bytes 190468
  7.2 27.9 %all-gather.2.cloned.1.call-start = ((), (), s32[]{:S(2)}) async-start(), calls=%async_computation.1 | async-start | bytes 3145728 | tf_op jit(solution)/shard_map/all_gather | solution.py:45
  7.9 35.4 %reduce-scatter.2.cloned.1.call-start = ((), (), s32[]{:S(2)}) async-start(), calls=%async_computation.2 | async-start | bytes 6291456 | tf_op jit(solution)/shard_map/reduce_scatter | solution.py:85
  8.7 7.7 %collective-permute-start.1 = (bf16[30,512]{1,0:T(8,128)(2,1)S(1)}, bf16[30,512]{1,0:T(8,128)(2,1)S(1)}, u32[]{:S(2)}, u32[]{:S(2)}) collective-permute-start(bf16[30,512]{1,0:T(8,128)(2,1)S(1)} %slice_bitcast_fusion), channel_id=1, source_target_pairs={{0,2},{2,4},{4,6},{6,8},{8,10},{10,12},{12,14},{14,16},{16,18},{18... | collective-permute-start | bytes 92168 | tf_op jit(solution)/shard_map/ppermute | solution.py:13
  12.9 7.6 %collective-permute-start = (bf16[30,512]{1,0:T(8,128)(2,1)S(1)}, bf16[30,512]{1,0:T(8,128)(2,1)S(1)}, u32[]{:S(2)}, u32[]{:S(2)}) collective-permute-start(bf16[30,512]{1,0:T(8,128)(2,1)S(1)} %slice_bitcast_fusion.1), channel_id=1, source_target_pairs={{0,2},{2,4},{4,6},{6,8},{8,10},{10,12},{12,14},{14,16},{16,18},{18... | collective-permute-start | bytes 92168 | tf_op jit(solution)/shard_map/ppermute | solution.py:13
  22.1 6.0 %copy-start.6 = (f32[512]{0:T(512)S(1)}, f32[512]{0:T(512)}, u32[]{:S(2)}) copy-start(f32[512]{0:T(512)} %param.11) | copy-start | bytes 6148
  22.2 6.0 %copy-start.7 = (f32[512]{0:T(512)S(1)}, f32[512]{0:T(512)}, u32[]{:S(2)}) copy-start(f32[512]{0:T(512)} %param.12) | copy-start | bytes 6148
  27.2 1.0 copy-start.2
  31.5 144.6 %all-reduce.4.cloned.1.call-start = ((), (), s32[]{:S(2)}) async-start(), calls=%async_computation.3 | async-start | bytes 4194304 | tf_op jit(solution)/shard_map/psum | solution.py:86
  31.6 2.4 copy-start.4
  43.3 262.5 %all-reduce.6.cloned.1.call-start = ((), (), s32[]{:S(2)}) async-start(), calls=%async_computation.4 | async-start | bytes 139264 | tf_op jit(solution)/shard_map/psum | solution.py:73
  47.6 6.8 %copy-start.1 = (f32[512,512]{1,0:T(8,128)}, f32[512,512]{1,0:T(8,128)S(1)}, u32[]{:S(2)}) copy-start(f32[512,512]{1,0:T(8,128)S(1)} %get-tuple-element.50) | copy-start | bytes 3145732
  47.6 10.3 %collective-permute-start.2 = (f32[30,512]{1,0:T(8,128)S(1)}, f32[30,512]{1,0:T(8,128)S(1)}, u32[]{:S(2)}, u32[]{:S(2)}) collective-permute-start(f32[30,512]{1,0:T(8,128)S(1)} %slice.489), channel_id=1, source_target_pairs={{2,0},{4,2},{6,4},{8,6},{10,8},{12,10},{14,12},{16,14},{18,16},{20... | collective-permute-start | bytes 184328 | tf_op jit(solution)/shard_map/ppermute | solution.py:13
  57.9 23.1 %copy-start.3 = (f32[542,512]{1,0:T(8,128)S(1)}, f32[542,512]{1,0:T(8,128)}, u32[]{:S(2)}) copy-start(f32[542,512]{1,0:T(8,128)} %maximum_convert_fusion.1) | copy-start | bytes 3330052
Sparse Core Ops, SparseCore 0:
  9.5 11.9 all-gather.1
  31.7 11.5 reduce-scatter.1
  48.8 127.2 all-reduce.3
  182.5 123.2 all-reduce.5
where the time goes:
time: 317 us; the launch traced here: 316 us
  waiting for transfers between devices  229 us (72%)
  other arithmetic  42.9 us (14%)
  between operations  14 us (4%)
  starting transfers between devices  11.4 us (4%)
  local copies, waits for them, and re-layouts  10.7 us (3%)
  matrix products  8.5 us (3%)
    psum x1, waiting for transfers between devices, per_device(): lax.psum((grad_taps * scale, jnp.sum(grad_pre * normed, axis=0) * scale,...  127 us
    psum x1, waiting for transfers between devices, per_device(): grad_out_weight = lax.psum(partial_rows, 'sp')  94.1 us
    broadcast_in_dim x1, other arithmetic, per_device(): grad_gate[None]  23 us
    ppermute x3, starting transfers between devices, from_behind(): return lax.ppermute(value, axis, pairs)  11.2 us
    unnamed x20, local copies, waits for them, and re-layouts  7.56 us
    reduce_sum x2, other arithmetic, per_device(): jnp.sum(grad_conv_rows * gated_ext[offset:offset + length], axis=0)  6.52 us
  transfers between devices with their start and end apart: 7, of which 4 were waited for; matrix products, arithmetic and copies ran while one was open for 18% of the time, Pallas kernels for 0%

commit v1 on v0

--- a/solution.py
+++ b/solution.py
@@ -83,7 +83,11 @@
         columns, act_rows, (((0,), (0,)), ((), ())), preferred_element_type=jnp.float32
     )
     partial_rows = lax.psum_scatter(product * scale, "dp", scatter_dimension=0, tiled=True)
-    grad_out_weight = lax.psum(partial_rows, "sp")
+    grad_out_weight = partial_rows
+    for hop in (1, 2, 4, 8):
+        grad_out_weight = grad_out_weight + lax.ppermute(
+            grad_out_weight, "sp", [(dev, dev ^ hop) for dev in range(16)]
+        )
     return (grad_value[None], grad_gate[None], grad_out_weight, grad_conv, grad_gain, grad_shift)
 
 

time: 317 us -> 396 us (1.25)
  waiting for transfers between devices: 229 us -> 302 us
  starting transfers between devices: 11.4 us -> 18.2 us
    ppermute x0 -> x4, waiting for transfers between devices: none -> 196 us  [per_device(): lax.ppermute(grad_out_weight, 'sp', [(dev, dev ^ hop) for dev in range(16)])]
    psum x1 -> x0, waiting for transfers between devices: 94.1 us -> none  [per_device(): grad_out_weight = lax.psum(partial_rows, 'sp')]
    psum x1, waiting for transfers between devices: 127 us -> 91.5 us  [per_device(): lax.psum((grad_taps * scale, jnp.sum(grad_pre * normed, axis=0) * scale,...]
    broadcast_in_dim x1, other arithmetic: 23 us -> 7.23 us  [per_device(): grad_gate[None]]
    add x0 -> x4, other arithmetic: none -> 15.6 us  [per_device(): grad_out_weight + lax.ppermute(grad_out_weight, 'sp', [(dev, dev ^ hop) f...]
    reduce_scatter x1, waiting for transfers between devices: 3.07 us -> 11.7 us  [per_device(): lax.psum_scatter(product * scale, 'dp', scatter_dimension=0, tiled=True)]
    ppermute x0 -> x4, starting transfers between devices: none -> 5.81 us  [per_device(): lax.ppermute(grad_out_weight, 'sp', [(dev, dev ^ hop) for dev in range(16)])]
  transfers between devices with their start and end apart: 7 -> 10, of which waited for: 4 -> 7; matrix products, arithmetic and copies ran while one was open for 18% -> 11% of each run, Pallas kernels for 0% -> 0%
where the time goes in v1:
time: 396 us; the launch traced here: 395 us
  waiting for transfers between devices  302 us (76%)
  other arithmetic  40.9 us (10%)
  starting transfers between devices  18.2 us (5%)
  between operations  13.9 us (4%)
  local copies, waits for them, and re-layouts  13 us (3%)
  matrix products  7.72 us (2%)
    ppermute x4, waiting for transfers between devices, per_device(): lax.ppermute(grad_out_weight, 'sp', [(dev, dev ^ hop) for dev in range(16)])  196 us
    psum x1, waiting for transfers between devices, per_device(): lax.psum((grad_taps * scale, jnp.sum(grad_pre * normed, axis=0) * scale,...  91.5 us
    add x4, other arithmetic, per_device(): grad_out_weight + lax.ppermute(grad_out_weight, 'sp', [(dev, dev ^ hop) f...  15.6 us
    ppermute x3, starting transfers between devices, from_behind(): return lax.ppermute(value, axis, pairs)  12.2 us
    reduce_scatter x1, waiting for transfers between devices, per_device(): lax.psum_scatter(product * scale, 'dp', scatter_dimension=0, tiled=True)  11.7 us
  transfers between devices with their start and end apart: 10, of which 7 were waited for; matrix products, arithmetic and copies ran while one was open for 11% of the time, Pallas kernels for 0%

profile of v1, /device:TPU:8, one launch (start us, length us, event | category | flops | bytes accessed | tf_op | source)
XLA Modules:
  0.0 395.5 jit_solution(1175594970375216227)
XLA Ops:
  7.2 0.0 copy-start
  7.2 0.0 reduce-scatter.2.cloned.1.call-start
  7.2 0.9 slice_bitcast_fusion
  8.1 3.4 collective-permute-start.1
  11.5 0.8 slice_bitcast_fusion.1
  12.3 3.4 collective-permute-start
  15.7 1.1 fusion.114
  16.9 1.0 fusion.115
  17.9 0.0 collective-permute-done.1
  17.9 2.0 collective-permute-done
  19.9 1.6 divide_multiply_fusion
  21.5 0.0 copy-start.7
  21.5 0.0 copy-start.10
  21.6 5.0 %fusion.113 = (f32[512]{0:T(512)S(1)}, f32[512,512]{1,0:T(8,128)S(1)}) fusion(f32[542,512]{1,0:T(8,128)S(1)} %divide_multiply_fusion, f32[512]{0:T(512)S(1)} %bitcast.148, f32[512]{0:T(512)S(1)} %bitcast.150, f32[512]{0:T(512)S(1)} %bitcast.92, f32[512]{0:T(512)S(1)} %bitcast.94, f32[512]{0:T(512)S(1)} %bitcast.96, f32[512]{0:T(512)S(1)} %bitcast.98, ...), kind=kLoop, calls=%fused_computation.212 | loop fusion | flops 16252416 | bytes 33619968 | tf_op jit(solution)/shard_map/reduce_sum | solution.py:36
  26.5 0.0 copy-start.3
  26.6 0.3 multiply_reduce_fusion.33
  26.8 0.7 copy-done.3
  27.5 0.0 copy-done
  27.5 0.0 copy-done.7
  27.5 0.0 copy-done.10
  27.6 3.4 multiply_bitcast_fusion
  30.9 0.0 reduce-scatter.2.cloned.1.call-update
  31.0 0.0 all-gather.2.cloned.1.call-start
  31.0 11.7 %reduce-scatter.2.cloned.1.call-done = f32[1024,512]{0,1:T(8,128)} async-done(((f32[2048,512]{0,1:T(8,128)}), f32[1024,512]{0,1:T(8,128)}) %reduce-scatter.2.cloned.1.call-update) | async-done | bytes 2097168 | tf_op jit(solution)/shard_map/reduce_scatter | solution.py:85
  42.7 1.5 collective-permute-start.3
  44.2 46.5 %collective-permute-done.3 = f32[1024,512]{0,1:T(8,128)S(1)} collective-permute-done((f32[1024,512]{0,1:T(8,128)}, f32[1024,512]{0,1:T(8,128)S(1)}, u32[]{:S(2)}, u32[]{:S(2)}) %collective-permute-start.3) | collective-permute-done | bytes 2097184 | tf_op jit(solution)/shard_map/ppermute | solution.py:88
  90.6 3.3 add.299
  93.9 1.5 collective-permute-start.4
  95.4 0.0 all-gather.2.cloned.1.call-update
  95.4 0.0 all-reduce.3.cloned.1.call-start
  95.5 0.0 copy-start.6
  95.5 2.3 maximum_convert_fusion.1
  97.7 0.0 copy-done.6
  97.8 1.2 maximum_convert_fusion
  98.9 42.2 %collective-permute-done.4 = f32[1024,512]{0,1:T(8,128)} collective-permute-done((f32[1024,512]{0,1:T(8,128)}, f32[1024,512]{0,1:T(8,128)}, u32[]{:S(2)}, u32[]{:S(2)}) %collective-permute-start.4) | collective-permute-done | bytes 2097184 | tf_op jit(solution)/shard_map/ppermute | solution.py:88
  141.1 4.1 %add.300 = f32[1024,512]{0,1:T(8,128)} add(f32[1024,512]{0,1:T(8,128)} %add.299, f32[1024,512]{0,1:T(8,128)} %collective-permute-done.4) | non-fusion elementwise | flops 524288 | bytes 6291456 | tf_op jit(solution)/shard_map/add | solution.py:88
  145.2 0.5 collective-permute-start.5
  145.7 4.3 %multiply_reduce_fusion = (f32[512]{0:T(512)}, f32[512]{0:T(512)S(1)}, f32[512]{0:T(512)S(1)}, f32[512]{0:T(512)}, f32[512,512]{1,0:T(8,128)S(1)}) fusion(f32[512,512]{1,0:T(8,128)} %copy-done.3, f32[512]{0:T(512)S(1)} %add_rsqrt_fusion, f32[512]{0:T(512)S(1)} %broadcast_multiply_fusion.5, f32[512]{0:T(512)S(1)} %copy-done.7, f32[512]{0:T(512)S(1)} %copy-done.10, ...), kind=kOutput, calls=%fused_computation.151 | convolution fusion | flops 1078720512 | bytes 6307840 | tf_op jit(solution)/shard_map/dot_general | solution.py:43
  150.0 0.0 copy-done.4
  150.0 3.2 multiply_reduce_fusion.1
  153.2 0.0 copy-start.1
  153.2 5.4 %collective-permute-start.2 = (f32[30,512]{1,0:T(8,128)S(1)}, f32[30,512]{1,0:T(8,128)S(1)}, u32[]{:S(2)}, u32[]{:S(2)}) collective-permute-start(f32[30,512]{1,0:T(8,128)S(1)} %slice.489), channel_id=1, source_target_pairs={{2,0},{4,2},{6,4},{8,6},{10,8},{12,10},{14,12},{16,14},{18,16},{20... | collective-permute-start | bytes 184328 | tf_op jit(solution)/shard_map/ppermute | solution.py:13
  158.7 2.3 multiply_reduce_fusion.19
  161.0 0.0 copy-done.1
  161.0 1.6 stack.127
  162.6 0.0 copy-start.8
  162.6 0.0 copy-start.9
  162.6 28.9 %collective-permute-done.5 = f32[1024,512]{0,1:T(8,128)} collective-permute-done((f32[1024,512]{0,1:T(8,128)}, f32[1024,512]{0,1:T(8,128)}, u32[]{:S(2)}, u32[]{:S(2)}) %collective-permute-start.5) | collective-permute-done | bytes 2097184 | tf_op jit(solution)/shard_map/ppermute | solution.py:88
  191.5 4.1 %add.301 = f32[1024,512]{0,1:T(8,128)} add(f32[1024,512]{0,1:T(8,128)} %add.300, f32[1024,512]{0,1:T(8,128)} %collective-permute-done.5) | non-fusion elementwise | flops 524288 | bytes 6291456 | tf_op jit(solution)/shard_map/add | solution.py:88
  195.6 2.4 collective-permute-start.6
  198.0 0.6 broadcast_multiply_fusion
  198.7 0.0 copy-done.8
  198.7 0.6 broadcast_multiply_fusion.1
  199.3 0.0 all-reduce.3.cloned.1.call-update
  199.3 0.0 collective-permute-done.2
  199.3 7.2 %fusion.105 = (bf16[1,512,512]{2,1,0:T(8,128)(2,1)}, f32[512,512]{1,0:T(8,128)S(1)}) fusion(f32[542,512]{1,0:T(8,128)} %maximum_convert_fusion, f32[542,512]{1,0:T(8,128)} %maximum_convert_fusion.1, f32[512,512]{1,0:T(8,128)S(1)} %copy-done.2, f32[512]{0:T(512)S(1)} %bitcast.149, f32[30,512]{1,0:T(8,128)S(1)} %collective-permute-done.2, ...), kind=kLoop, calls=%fused_computation.196 | loop fusion | flops 25952256 | bytes 4843520 | tf_op jit(solution)/shard_map/broadcast_in_dim | solution.py:91
  206.5 1.1 fusion.104
  207.6 78.9 %collective-permute-done.6 = f32[1024,512]{0,1:T(8,128)} collective-permute-done((f32[1024,512]{0,1:T(8,128)}, f32[1024,512]{0,1:T(8,128)}, u32[]{:S(2)}, u32[]{:S(2)}) %collective-permute-start.6) | collective-permute-done | bytes 2097184 | tf_op jit(solution)/shard_map/ppermute | solution.py:88
  286.5 4.1 %add.302 = f32[1024,512]{0,1:T(8,128)} add(f32[1024,512]{0,1:T(8,128)} %add.301, f32[1024,512]{0,1:T(8,128)} %collective-permute-done.6) | non-fusion elementwise | flops 524288 | bytes 6291456 | tf_op jit(solution)/shard_map/add | solution.py:88
  290.6 2.9 copy.13
  293.4 91.5 %all-reduce.3.cloned.1.call-done = (f32[31,512]{1,0:T(8,128)}, f32[512]{0:T(512)}, f32[512]{0:T(512)}) async-done(((f32[31,512]{1,0:T(8,128)}, f32[512]{0:T(512)}, f32[512]{0:T(512)}), (f32[31,512]{1,0:T(8,128)}, f32[512]{0:T(512)}, f32[512]{0:T(512)})) %all-reduce.3.cloned.1.call-update) | async-done | bytes 67600 | tf_op jit(solution)/shard_map/psum | solution.py:73
  385.0 1.5 copy.17
  386.5 1.2 copy.18
  387.7 1.2 copy.19
  (11 shorter events, 0.0 us)
Async XLA Ops:
  7.2 20.4 %copy-start = (bf16[1,512,2048]{2,1,0:T(8,128)(2,1)S(1)}, bf16[1,512,2048]{2,1,0:T(8,128)(2,1)}, u32[]{:S(2)}) copy-start(bf16[1,512,2048]{2,1,0:T(8,128)(2,1)} %param.9) | copy-start | bytes 6291460
  7.2 35.5 %reduce-scatter.2.cloned.1.call-start = ((), (), s32[]{:S(2)}) async-start(), calls=%async_computation.2 | async-start | bytes 6291456 | tf_op jit(solution)/shard_map/reduce_scatter | solution.py:85
  8.1 9.8 %collective-permute-start.1 = (bf16[30,512]{1,0:T(8,128)(2,1)S(1)}, bf16[30,512]{1,0:T(8,128)(2,1)S(1)}, u32[]{:S(2)}, u32[]{:S(2)}) collective-permute-start(bf16[30,512]{1,0:T(8,128)(2,1)S(1)} %slice_bitcast_fusion), channel_id=1, source_target_pairs={{0,2},{2,4},{4,6},{6,8},{8,10},{10,12},{12,14},{14,16},{16,18},{18... | collective-permute-start | bytes 92168 | tf_op jit(solution)/shard_map/ppermute | solution.py:13
  12.3 7.6 %collective-permute-start = (bf16[30,512]{1,0:T(8,128)(2,1)S(1)}, bf16[30,512]{1,0:T(8,128)(2,1)S(1)}, u32[]{:S(2)}, u32[]{:S(2)}) collective-permute-start(bf16[30,512]{1,0:T(8,128)(2,1)S(1)} %slice_bitcast_fusion.1), channel_id=1, source_target_pairs={{0,2},{2,4},{4,6},{6,8},{8,10},{10,12},{12,14},{14,16},{16,18},{18... | collective-permute-start | bytes 92168 | tf_op jit(solution)/shard_map/ppermute | solution.py:13
  21.5 6.0 %copy-start.7 = (f32[512]{0:T(512)S(1)}, f32[512]{0:T(512)}, u32[]{:S(2)}) copy-start(f32[512]{0:T(512)} %param.11) | copy-start | bytes 6148
  21.5 6.0 %copy-start.10 = (f32[512]{0:T(512)S(1)}, f32[512]{0:T(512)}, u32[]{:S(2)}) copy-start(f32[512]{0:T(512)} %param.12) | copy-start | bytes 6148
  26.5 1.0 copy-start.3
  31.0 114.7 %all-gather.2.cloned.1.call-start = ((), (), s32[]{:S(2)}) async-start(), calls=%async_computation.1 | async-start | bytes 3145728 | tf_op jit(solution)/shard_map/all_gather | solution.py:45
  42.7 47.9 %collective-permute-start.3 = (f32[1024,512]{0,1:T(8,128)}, f32[1024,512]{0,1:T(8,128)S(1)}, u32[]{:S(2)}, u32[]{:S(2)}) collective-permute-start(f32[1024,512]{0,1:T(8,128)} %reduce-scatter.2.cloned.1.call-done), channel_id=1, source_target_pairs={{0,2},{2,0},{4,6},{6,4},{8,10},{10,8},{12,14},{14,12},{16,18},{18,... | collective-permute-start | bytes 6291464 | tf_op jit(solution)/shard_map/ppermute | solution.py:88
  93.9 47.2 %collective-permute-start.4 = (f32[1024,512]{0,1:T(8,128)}, f32[1024,512]{0,1:T(8,128)}, u32[]{:S(2)}, u32[]{:S(2)}) collective-permute-start(f32[1024,512]{0,1:T(8,128)} %add.299), channel_id=1, source_target_pairs={{0,4},{2,6},{4,0},{6,2},{8,12},{10,14},{12,8},{14,10},{16,20},{18,... | collective-permute-start | bytes 6291464 | tf_op jit(solution)/shard_map/ppermute | solution.py:88
  95.4 289.5 %all-reduce.3.cloned.1.call-start = ((), (), s32[]{:S(2)}) async-start(), calls=%async_computation.3 | async-start | bytes 139264 | tf_op jit(solution)/shard_map/psum | solution.py:73
  95.5 2.3 copy-start.6
  145.2 46.3 %collective-permute-start.5 = (f32[1024,512]{0,1:T(8,128)}, f32[1024,512]{0,1:T(8,128)}, u32[]{:S(2)}, u32[]{:S(2)}) collective-permute-start(f32[1024,512]{0,1:T(8,128)} %add.300), channel_id=1, source_target_pairs={{0,8},{2,10},{4,12},{6,14},{8,0},{10,2},{12,4},{14,6},{16,24},{18,... | collective-permute-start | bytes 6291464 | tf_op jit(solution)/shard_map/ppermute | solution.py:88
  145.7 4.3 %copy-start.4 = (f32[512,512]{1,0:T(8,128)S(1)}, f32[512,512]{1,0:T(8,128)}, u32[]{:S(2)}) copy-start(f32[512,512]{1,0:T(8,128)} %copy-done.3) | copy-start | bytes 3145732
  153.2 7.8 %copy-start.1 = (f32[512,512]{1,0:T(8,128)}, f32[512,512]{1,0:T(8,128)S(1)}, u32[]{:S(2)}) copy-start(f32[512,512]{1,0:T(8,128)S(1)} %get-tuple-element.50) | copy-start | bytes 3145732
  153.2 46.1 %collective-permute-start.2 = (f32[30,512]{1,0:T(8,128)S(1)}, f32[30,512]{1,0:T(8,128)S(1)}, u32[]{:S(2)}, u32[]{:S(2)}) collective-permute-start(f32[30,512]{1,0:T(8,128)S(1)} %slice.489), channel_id=1, source_target_pairs={{2,0},{4,2},{6,4},{8,6},{10,8},{12,10},{14,12},{16,14},{18,16},{20... | collective-permute-start | bytes 184328 | tf_op jit(solution)/shard_map/ppermute | solution.py:13
  162.6 36.1 %copy-start.8 = (f32[512]{0:T(512)S(1)}, f32[512]{0:T(512)}, u32[]{:S(2)}) copy-start(f32[512]{0:T(512)} %get-tuple-element.43) | copy-start | bytes 6148
  162.6 36.1 %copy-start.9 = (f32[512]{0:T(512)S(1)}, f32[512]{0:T(512)}, u32[]{:S(2)}) copy-start(f32[512]{0:T(512)} %get-tuple-element.46) | copy-start | bytes 6148
  162.6 36.7 %copy-start.2 = (f32[512,512]{1,0:T(8,128)S(1)}, f32[512,512]{1,0:T(8,128)}, u32[]{:S(2)}) copy-start(f32[512,512]{1,0:T(8,128)} %copy-done.1) | copy-start | bytes 3145732
  195.6 90.9 %collective-permute-start.6 = (f32[1024,512]{0,1:T(8,128)}, f32[1024,512]{0,1:T(8,128)}, u32[]{:S(2)}, u32[]{:S(2)}) collective-permute-start(f32[1024,512]{0,1:T(8,128)} %add.301), channel_id=1, source_target_pairs={{0,16},{2,18},{4,20},{6,22},{8,24},{10,26},{12,28},{14,30},{16,0},... | collective-permute-start | bytes 6291464 | tf_op jit(solution)/shard_map/ppermute | solution.py:88
  199.3 7.3 %copy-start.5 = (f32[542,512]{1,0:T(8,128)S(1)}, f32[542,512]{1,0:T(8,128)}, u32[]{:S(2)}) copy-start(f32[542,512]{1,0:T(8,128)} %maximum_convert_fusion.1) | copy-start | bytes 3330052
Sparse Core Ops, SparseCore 0:
  31.1 11.5 reduce-scatter.1
  95.5 10.8 all-gather.1
  199.4 185.5 all-reduce.2
